TPU v7x, 512 devices: a 8x2x16 block of a 8x8x16 slice. The times are simulated.
512 devices in a mesh: grp: 2 (over y), ep: 32 (over z, core), tp: 8 (over x).
Axes of the slice: x: 8, y: 2, z: 16, core: 2. Of those that a mesh axis runs over, the one named last changes fastest.
The devices are a block of a 8x8x16 slice.
Arguments:
- tokens: bfloat16 [4096, 4096], P(('grp', 'ep'), 'tp'), parts along dimension 0, may hold values from -27 to 27
- group_choice: int32 [4096], P(('grp', 'ep')), parts along dimension 0, may hold values from 0 to 3, as said below
- member_choice: int32 [4096, 4], P(('grp', 'ep')), parts along dimension 0, may hold values from 0 to 7, as said below
- group_prob: float32 [4096], P(('grp', 'ep')), parts along dimension 0, may hold values from 0.3 to 1
- member_score: float32 [4096, 4], P(('grp', 'ep')), parts along dimension 0, may hold values from -4 to 4
- norm_gain: float32 [4096], P('tp'), may hold values from 0.1 to 1.9
- w_gate: bfloat16 [32, 4096, 1024], P('ep', 'tp'), may hold values from -0.09375 to 0.09375
- w_up: bfloat16 [32, 4096, 1024], P('ep', 'tp'), may hold values from -0.09375 to 0.09375
- w_down: bfloat16 [32, 1024, 4096], P('ep', None, 'tp'), may hold values from -0.1875 to 0.1875
- final_gain: float32 [4096], P('tp'), may hold values from 0.1 to 1.9
Outputs:
- mixed: bfloat16 [4096, 4096], P(('grp', 'ep'), 'tp'), parts along dimension 0
There are 2 independent parts, one for each index of `grp`. A program takes and returns all parts, laid end to end along the dimension named above; an argument that names none is the same for every part. Nothing has to cross between parts.
Inputs may be any that keep to these rules, and one draw needn't show every extreme that they name: `group_choice`: in each aligned block of 64 tokens every group is chosen by exactly 16 tokens. `member_choice`: each row names 4 different experts of its token's group. In each aligned block of 64 rows no expert (group and member together) is named by more than 16 rows, some expert is named by exactly 16 rows, and one expert is named by exactly 16 rows in every block.
All inputs are finite; a program needn't handle non-finite values.
Results may differ from a plain program's by a relative error of at most 0.017.
Values may be sent and summed in bfloat16 or wider, within the bound.
A program may use at most 64 MiB of HBM per device.

v0:
```python
import jax
import jax.numpy as jnp
from jax import lax
from jax.sharding import Mesh
from jax.sharding import PartitionSpec as P

EP = ("ep_0", "ep_1")
GRP_EP = ("grp", "ep_0", "ep_1")


EPS = 1e-06


def in_blocks(value, dim, devices):
    before, after = (value.shape[:dim], value.shape[dim + 1 :])
    return jnp.moveaxis(value.reshape(*before, devices, -1, *after), dim, 0)


def sum_together(arrays, axis, dims):
    devices = lax.axis_size(axis)
    pieces = [in_blocks(a, dim, devices) for a, dim in zip(arrays, dims)]
    lines = jnp.concatenate([b.reshape(devices, -1) for b in pieces], axis=1)
    extent = max(16, -(-lines.shape[1] // 1024) * 8)
    lines = jnp.pad(lines, ((0, 0), (0, extent * 128 - lines.shape[1]))).reshape(-1, 128)
    vector, at, gathered = (lax.psum_scatter(lines, axis, tiled=True).reshape(-1), 0, [])
    for b in pieces:
        part = b[0]
        gathered.append(vector[at : at + part.size].reshape(part.shape))
        at += part.size
    return tuple(gathered)


def copy_for_each(value, axis):
    copies = jnp.broadcast_to(value, (lax.axis_size(axis), *value.shape))
    return lax.all_to_all(copies, axis, split_axis=0, concat_axis=0, tiled=True)


def in_order(pieces, dim):
    pieces = jnp.moveaxis(pieces, 0, dim)
    shape = pieces.shape
    return pieces.reshape(*shape[:dim], shape[dim] * shape[dim + 1], *shape[dim + 2 :])


def collect(value, axis, dim):
    pieces = copy_for_each(value, axis)
    return in_order(pieces, dim)


def over_copies(value, axis):
    return copy_for_each(value, axis).sum(axis=0)


def turned_blocks(pieces, axes, order):
    inside = pieces.shape[1:]
    whole = pieces.reshape(*(lax.axis_size(a) for a in axes), *inside)
    for k in order:
        whole = lax.all_to_all(whole, axes[k], k, k, tiled=True)
    return whole.reshape(-1, *inside)


def core_and_chips(value, groups, order, split_dim, concat_dim):
    devices = lax.axis_size(groups[0]) * lax.axis_size(groups[1])
    pieces = in_blocks(value, split_dim, devices)
    return in_order(turned_blocks(pieces, groups, order), concat_dim)


def slot_table(expert_ids, experts, capacity):
    flat_ids = expert_ids.reshape(-1)
    onehot = (flat_ids[:, None] == jnp.arange(experts, dtype=jnp.int32)[None, :]).astype(jnp.int32)
    before = jnp.cumsum(onehot, axis=0) - onehot
    position = jnp.sum(before * onehot, axis=1)
    return (flat_ids * capacity + position).reshape(expert_ids.shape)


def expert_rows(rows_in, gate_w, up_w, down_w):
    gate_part = jnp.dot(rows_in, gate_w, preferred_element_type=jnp.float32)
    up_part = jnp.dot(rows_in, up_w, preferred_element_type=jnp.float32)
    gate_cols, up_cols = tuple(
        (
            part.astype(jnp.float32)
            for part in sum_together(
                (gate_part.astype(jnp.bfloat16), up_part.astype(jnp.bfloat16)), "tp", (1, 1)
            )
        )
    )
    hidden_part = (jax.nn.silu(gate_cols) * up_cols).astype(jnp.bfloat16)
    hidden = collect(hidden_part, "tp", 1)
    return jnp.dot(hidden, down_w, preferred_element_type=jnp.float32).astype(jnp.bfloat16)


def local(
    tokens,
    group_choice,
    member_choice,
    group_prob,
    member_score,
    norm_gain,
    w_gate,
    w_up,
    w_down,
    final_gain,
):
    experts = lax.axis_size(EP)
    groups = max(2, experts // 8)
    per_group = experts // groups
    tok_dev = tokens.shape[0]
    capacity = tok_dev // groups
    full_width = tokens.shape[1] * lax.axis_size("tp")
    gate_w = w_gate[0]
    up_w = w_up[0]
    down_w = w_down[0]
    values = tokens.astype(jnp.float32)
    square_in = over_copies(jnp.sum(values * values, axis=1), "tp")
    normed = (
        values * lax.rsqrt(square_in[:, None] / full_width + EPS) * norm_gain[None, :]
    ).astype(jnp.bfloat16)
    expert_ids = group_choice[:, None] * per_group + member_choice
    scores = jnp.exp(member_score)
    weights = group_prob[:, None] * scores / jnp.sum(scores, axis=1, keepdims=True)
    destination = slot_table(expert_ids, experts, capacity)
    slot_iota = jnp.arange(experts * capacity, dtype=jnp.int32)
    picker = (destination[:, :, None] == slot_iota[None, None, :]).astype(jnp.bfloat16)
    outgoing = jnp.einsum("tkr,td->rd", picker, normed, preferred_element_type=jnp.float32).astype(
        jnp.bfloat16
    )
    outgoing = outgoing.reshape(experts, capacity, -1)
    received = lax.all_to_all(outgoing, EP, split_axis=0, concat_axis=0, tiled=True)
    produced = expert_rows(received.reshape(-1, received.shape[2]), gate_w, up_w, down_w)
    returned = core_and_chips(produced.reshape(received.shape), ("ep_0", "ep_1"), (1, 0), 0, 0)
    picked_rows = jnp.einsum(
        "tkr,rd->tkd",
        picker,
        returned.reshape(experts * capacity, -1),
        preferred_element_type=jnp.float32,
    )
    moe = jnp.sum(weights[:, :, None] * picked_rows, axis=1)
    summed = values + moe
    square_out = over_copies(jnp.sum(summed * summed, axis=1), "tp")
    return (
        summed * lax.rsqrt(square_out[:, None] / full_width + EPS) * final_gain[None, :]
    ).astype(jnp.bfloat16)


def solution(mesh):
    finer = Mesh(
        mesh.devices.reshape(mesh.shape["grp"], 16, 2, mesh.shape["tp"]),
        ("grp", "ep_0", "ep_1", "tp"),
    )
    placed = (
        P(GRP_EP, "tp"),
        P(GRP_EP),
        P(GRP_EP, None),
        P(GRP_EP),
        P(GRP_EP, None),
        P("tp"),
        P(EP, "tp", None),
        P(EP, "tp", None),
        P(EP, None, "tp"),
        P("tp"),
    )
    return jax.shard_map(
        local, mesh=finer, in_specs=placed, out_specs=P(GRP_EP, "tp"), check_vma=False
    )
```

profile of v0, /device:TPU:80, one launch (start us, length us, event | category | flops | bytes accessed | tf_op | source)
XLA Modules:
  0.0 239.3 jit_solution(14317533975861085024)
XLA Ops:
  6.6 1.0 fusion.13
  7.6 0.6 broadcast_in_dim.6
  8.2 7.3 %all-to-all-start = ((f32[8,1,64]{2,1,0:T(1,128)}), f32[8,1,64]{2,1,0:T(1,128)S(1)}, u32[]{:S(2)}, u32[]{:S(2)}) async-start(f32[8,1,64]{2,1,0:T(1,128)} %broadcast_in_dim.6), calls=%async_computation | async-start | bytes 8192 | tf_op jit(solution)/shard_map/all_to_all | solution.py:35
  15.6 0.8 copy.30
  16.4 0.7 broadcast_multiply_fusion
  17.3 0.6 reduce-window.6
  17.9 0.2 slice_reduce_fusion
  18.3 0.1 reduce_sum.76
  18.5 0.1 convert_reduce_fusion
  18.7 4.5 %all-to-all-done = f32[8,1,64]{2,1,0:T(1,128)S(1)} async-done(((f32[8,1,64]{2,1,0:T(1,128)}), f32[8,1,64]{2,1,0:T(1,128)S(1)}, u32[]{:S(2)}, u32[]{:S(2)}) %all-to-all-start) | async-done | bytes 2080 | tf_op jit(solution)/shard_map/all_to_all | solution.py:35
  23.2 1.2 convolution_convert_fusion.3
  24.4 77.3 %all_to_all.32 = bf16[32,16,512]{2,1,0:T(8,128)(2,1)S(1)} all-to-all(bf16[32,16,512]{2,1,0:T(8,128)(2,1)S(1)} %bitcast.60), channel_id=1, replica_groups=mesh['grp'=2,'ep_0'=16,'ep_1'=2,'tp'=8] {'ep_0','ep_1'}, dimensions={0} | all-to-all | bytes 1048576 | tf_op jit(solution)/shard_map/all_to_all | solution.py:127
  101.7 0.7 fusion
  102.4 0.3 copy.39
  102.7 0.2 copy-done.5
  103.0 0.7 fusion.1
  103.7 0.3 copy.40
  103.9 0.1 pad_maximum_fusion
  104.1 2.3 reshape.93
  106.5 35.6 %reduce-scatter.2.cloned.1.call-done = bf16[1024,128]{1,0:T(8,128)(2,1)} async-done(((bf16[8192,128]{1,0:T(8,128)(2,1)}), bf16[1024,128]{1,0:T(8,128)(2,1)}) %reduce-scatter.2.cloned.1.call-update) | async-done | bytes 262160 | tf_op jit(solution)/shard_map/reduce_scatter | solution.py:25
  142.0 1.1 fusion.12
  143.1 0.1 copy.34
  143.3 29.5 %all_to_all.33 = bf16[8,512,128]{1,2,0:T(8,128)(2,1)S(1)} all-to-all(bf16[8,512,128]{1,2,0:T(8,128)(2,1)S(1)} %broadcast_in_dim.7), channel_id=1, replica_groups=mesh['grp'=2,'ep_0'=16,'ep_1'=2,'tp'=8] {'tp'}, dimensions={0} | all-to-all | bytes 2097152 | tf_op jit(solution)/shard_map/all_to_all | solution.py:35
  172.8 0.7 convolution_convert_fusion.2
  173.7 4.3 %all_to_all.34 = bf16[16,2,1,16,512]{4,3,0,2,1:T(8,128)(2,1)S(1)} all-to-all(bf16[16,2,1,16,512]{4,3,0,2,1:T(8,128)(2,1)S(1)} %copy.35), channel_id=1, replica_groups=mesh['grp'=2,'ep_0'=16,'ep_1'=2,'tp'=8] {'ep_1'}, dimensions={1} | all-to-all | bytes 1048576 | tf_op jit(solution)/shard_map/all_to_all | solution.py:57
  178.0 0.8 copy.36
  178.8 13.3 %all-to-all-start.4 = ((bf16[16,2,1,16,512]{4,3,1,2,0:T(8,128)(2,1)}), bf16[16,2,1,16,512]{4,3,1,2,0:T(8,128)(2,1)S(1)}, u32[]{:S(2)}, u32[]{:S(2)}) async-start(bf16[16,2,1,16,512]{4,3,1,2,0:T(8,128)(2,1)} %copy.36), calls=%async_computation.5 | async-start | bytes 1048576 | tf_op jit(solution)/shard_map/all_to_all | solution.py:57
  192.2 29.0 %all-to-all-done.4 = bf16[16,2,1,16,512]{4,3,1,2,0:T(8,128)(2,1)S(1)} async-done(((bf16[16,2,1,16,512]{4,3,1,2,0:T(8,128)(2,1)}), bf16[16,2,1,16,512]{4,3,1,2,0:T(8,128)(2,1)S(1)}, u32[]{:S(2)}, u32[]{:S(2)}) %all-to-all-start.4) | async-done | bytes 524320 | tf_op jit(solution)/shard_map/all_to_all | solution.py:57
  221.1 0.4 fusion.2
  221.5 0.1 multiply_reduce_fusion
  221.6 10.1 %all_to_all.35 = f32[8,1,64]{2,1,0:T(1,128)S(1)} all-to-all(f32[8,1,64]{2,1,0:T(1,128)S(1)} %broadcast_in_dim.8), channel_id=1, replica_groups=mesh['grp'=2,'ep_0'=16,'ep_1'=2,'tp'=8] {'tp'}, dimensions={0} | all-to-all | bytes 4096 | tf_op jit(solution)/shard_map/all_to_all | solution.py:35
  231.8 0.7 multiply_convert_fusion
  (33 shorter events, 0.9 us)
Async XLA Ops:
  6.5 95.2 %copy-start = (bf16[1,512,1024]{2,1,0:T(8,128)(2,1)S(1)}, bf16[1,512,1024]{2,1,0:T(8,128)(2,1)}, u32[]{:S(2)}) copy-start(bf16[1,512,1024]{2,1,0:T(8,128)(2,1)} %param.16) | copy-start | bytes 3145732
  8.2 14.9 %all-to-all-start = ((f32[8,1,64]{2,1,0:T(1,128)}), f32[8,1,64]{2,1,0:T(1,128)S(1)}, u32[]{:S(2)}, u32[]{:S(2)}) async-start(f32[8,1,64]{2,1,0:T(1,128)} %broadcast_in_dim.6), calls=%async_computation | async-start | bytes 8192 | tf_op jit(solution)/shard_map/all_to_all | solution.py:35
  15.5 126.5 %reduce-scatter.2.cloned.1.call-start = ((), (), s32[]{:S(2)}) async-start(), calls=%async_computation.7 | async-start | bytes 2359296 | tf_op jit(solution)/shard_map/reduce_scatter | solution.py:25
  101.7 1.2 copy-start.5
  106.5 66.4 %copy-start.6 = (bf16[1,1024,512]{2,1,0:T(8,128)(2,1)S(1)}, bf16[1,1024,512]{2,1,0:T(8,128)(2,1)}, u32[]{:S(2)}) copy-start(bf16[1,1024,512]{2,1,0:T(8,128)(2,1)} %param.18) | copy-start | bytes 3145732
  173.6 18.5 %copy-start.2 = (f32[64,4]{0,1:T(4,128)S(1)}, f32[64,4]{0,1:T(4,128)}, u32[]{:S(2)}) copy-start(f32[64,4]{0,1:T(4,128)} %param.14) | copy-start | bytes 3076
  173.6 18.6 %copy-start.4 = (f32[64]{0:T(128)S(1)}, f32[64]{0:T(128)}, u32[]{:S(2)}) copy-start(f32[64]{0:T(128)} %param.13) | copy-start | bytes 772
  173.6 47.9 %copy-start.1 = (bf16[64,512]{1,0:T(8,128)(2,1)S(1)}, bf16[64,512]{1,0:T(8,128)(2,1)}, u32[]{:S(2)}) copy-start(bf16[64,512]{1,0:T(8,128)(2,1)} %param.10) | copy-start | bytes 196612
  173.6 58.1 %copy-start.3 = (f32[512]{0:T(512)S(1)}, f32[512]{0:T(512)}, u32[]{:S(2)}) copy-start(f32[512]{0:T(512)} %param.19) | copy-start | bytes 6148
  178.8 42.3 %all-to-all-start.4 = ((bf16[16,2,1,16,512]{4,3,1,2,0:T(8,128)(2,1)}), bf16[16,2,1,16,512]{4,3,1,2,0:T(8,128)(2,1)S(1)}, u32[]{:S(2)}, u32[]{:S(2)}) async-start(bf16[16,2,1,16,512]{4,3,1,2,0:T(8,128)(2,1)} %copy.36), calls=%async_computation.5 | async-start | bytes 1048576 | tf_op jit(solution)/shard_map/all_to_all | solution.py:57
Sparse Core Ops, SparseCore 0:
  106.6 35.4 reduce-scatter.1
where the time goes:
time: 240 us; the launch traced here: 239 us
  blocking collectives  121 us (50%)
  waiting for transfers between devices  69.1 us (29%)
  starting transfers between devices  20.7 us (9%)
  between operations  13.6 us (6%)
  local copies, waits for them, and re-layouts  6.13 us (3%)
  other arithmetic  4.83 us (2%)
  matrix products  3.69 us (2%)
    all_to_all x1, blocking collectives, local(): lax.all_to_all(outgoing, EP, split_axis=0, concat_axis=0, tiled=True)  77.3 us
    all_to_all x2, blocking collectives, copy_for_each(): return lax.all_to_all(copies, axis, split_axis=0, concat_axis=0, tiled=True)  39.6 us
    reduce_scatter x1, waiting for transfers between devices, sum_together(): lax.psum_scatter(lines, axis, tiled=True).reshape(-1)  35.6 us
    all_to_all x1, waiting for transfers between devices, turned_blocks(): whole = lax.all_to_all(whole, axes[k], k, k, tiled=True)  29 us
    all_to_all x1, starting transfers between devices, turned_blocks(): whole = lax.all_to_all(whole, axes[k], k, k, tiled=True)  13.3 us
    all_to_all x1, starting transfers between devices, copy_for_each(): return lax.all_to_all(copies, axis, split_axis=0, concat_axis=0, tiled=True)  7.32 us
  transfers between devices with their start and end apart: 3, of which 3 were waited for; matrix products, arithmetic and copies ran while one was open for 1% of the time, Pallas kernels for 0%

commit v1 on v0

v1 whole, which is shorter than its diff:
```python
import functools

import jax
import jax.numpy as jnp
from jax import lax
from jax.experimental import pallas as pl
from jax.experimental.pallas import tpu as pltpu
from jax.sharding import PartitionSpec as P

EPS = 1e-06
F32 = jnp.float32
BF16 = jnp.bfloat16
MESH = pl.DeviceIdType.MESH

CHUNKS = ((1, -1, 2, 0), (-2, 3, -3, 4), (7, -7, 8, -6), (-4, 5, -5, 6))
START = (0, 2, 4, 6)


def dot(a, b):
    return jnp.dot(a, b, preferred_element_type=F32)


def iota(shape, dim):
    return lax.broadcasted_iota(jnp.int32, shape, dim)


def column_of(row, n):
    shape = (n, row.shape[1])
    same = iota(shape, 0) == iota(shape, 1)
    return jnp.sum(jnp.where(same, jnp.broadcast_to(row, shape), 0.0), axis=1, keepdims=True)


def row_of(column, lanes):
    shape = (column.shape[0], lanes)
    same = iota(shape, 0) == iota(shape, 1)
    return jnp.sum(jnp.where(same, jnp.broadcast_to(column, shape), 0.0), axis=0, keepdims=True)


def split3(value):
    first = value.astype(BF16).astype(F32)
    rest = value - first
    second = rest.astype(BF16).astype(F32)
    third = (rest - second).astype(BF16).astype(F32)
    return first, second, third


def kernel(
    dims,
    tokens_ref,
    group_ref,
    member_ref,
    prob_ref,
    score_ref,
    gain_ref,
    final_ref,
    wg_ref,
    wu_ref,
    wd_ref,
    out_ref,
    wgu,
    wdn,
    sorted_buf,
    meta_src,
    rows,
    meta,
    sq_buf,
    sq2_buf,
    rs_send,
    rs_recv,
    hid,
    kept,
    pair_send,
    pair_recv,
    ret_send,
    ret_recv,
    w_sem,
    z_send,
    z_recv,
    m_recv,
    fwd_send,
    fwd_recv,
    mfwd_send,
    mfwd_recv,
    sq_send,
    sq_recv,
    rs_ssem,
    rs_rsem,
    ag_ssem,
    ag_rsem,
    pair_ssem,
    pair_rsem,
    r_recv,
):
    n_z, n_x, groups, width = dims
    per_chips = n_z // groups
    tok, dl = tokens_ref.shape
    cap = tok // groups
    half = n_x // 2
    cols = wgu.shape[2] // 2
    n_rows = rows.shape[1]
    n_mine = n_rows // 2
    ep, me = lax.axis_index("ep"), lax.axis_index("tp")
    z, core = lax.div(ep, 2), lax.rem(ep, 2)
    partner = {"ep": 2 * z + 1 - core}
    right = {"tp": lax.rem(me + 1, n_x)}
    left = {"tp": lax.rem(me + n_x - 1, n_x)}

    def chip(offset):
        return lax.rem(z + offset + n_z, n_z)

    def at_chip(offset):
        return {"ep": 2 * chip(offset) + core}

    def peer(offset):
        return {"tp": lax.rem(me + offset + n_x, n_x)}

    def x_index(offset):
        return lax.rem(me + offset + n_x, n_x)

    def send(src, dst, ssem, rsem, device):
        pltpu.make_async_remote_copy(
            src_ref=src, dst_ref=dst, send_sem=ssem, recv_sem=rsem, device_id=device, device_id_type=MESH
        ).start()

    def await_bytes(ref, sem):
        pltpu.make_async_copy(ref, ref, sem).wait()

    barrier = pltpu.get_barrier_semaphore()
    greeted = [at_chip(k) for k in range(1, n_z)] + [partner] + [peer(k) for k in range(1, n_x)]
    for device in greeted:
        pl.semaphore_signal(barrier, inc=1, device_id=device, device_id_type=MESH)

    loads = []
    for o in range(n_x):
        span = pl.ds(o * cols, cols)
        loads.append(pltpu.make_async_copy(wg_ref.at[0, :, span], wgu.at[o, :, pl.ds(0, cols)], w_sem.at[0]))
        loads.append(pltpu.make_async_copy(wu_ref.at[0, :, span], wgu.at[o, :, pl.ds(cols, cols)], w_sem.at[0]))
    loads.append(pltpu.make_async_copy(wd_ref.at[0], wdn, w_sem.at[1]))
    for load in loads:
        load.start()

    values = tokens_ref[...].astype(F32)
    scaled = (values * gain_ref[...]).astype(BF16)
    group_row = group_ref[...]
    chosen = (iota((8, tok), 0) == jnp.broadcast_to(group_row, (8, tok))).astype(F32)
    earlier = (iota((tok, tok), 0) < iota((tok, tok), 1)).astype(F32)
    rank = jnp.sum(dot(chosen, earlier) * chosen, axis=0, keepdims=True)
    slot_row = group_row.astype(F32) * cap + rank
    slot_col = column_of(slot_row, tok)
    picker = (iota((tok, tok), 0).astype(F32) == jnp.broadcast_to(slot_row, (tok, tok))).astype(BF16)
    sorted_buf[...] = dot(picker, scaled).astype(BF16)
    square = jnp.sum(values * values, axis=1, keepdims=True)
    sq_buf[pl.ds(me, 1)] = row_of(square, 128).reshape(1, 1, 128)

    def block_of(offset):
        g = lax.div(chip(-offset), per_chips)
        return pl.ds(pl.multiple_of(g * cap, cap), cap)

    pl.semaphore_wait(barrier, len(greeted))

    for c, offsets in enumerate(CHUNKS):
        for j, offset in enumerate(offsets):
            place = pl.ds(j * cap, cap)
            if offset == 0:
                rows[c, place, :] = sorted_buf[block_of(0), :]
            else:
                send(sorted_buf.at[block_of(offset)], rows.at[c, place], z_send.at[0], z_recv.at[c], at_chip(-offset))
    for k in range(1, n_x):
        send(sq_buf.at[me], sq_buf.at[me], sq_send.at[0], sq_recv.at[0], peer(k))

    def remote_rows(c):
        return pl.ds(0, cap * sum(1 for offset in CHUNKS[c] if offset != 0))

    def take(c):
        await_bytes(rows.at[c, remote_rows(c)], z_recv.at[c])
        send(rows.at[c, pl.ds(0, n_mine)], rows.at[c, pl.ds(n_mine, n_mine)], fwd_send.at[c], fwd_recv.at[c], partner)

    def send_meta():
        await_bytes(sq_buf.at[pl.ds(0, n_x - 1)], sq_recv.at[0])
        total = column_of(jnp.sum(sq_buf[...], axis=0), tok)
        factor = lax.rsqrt(total / width + EPS)
        score = jnp.exp(score_ref[...])
        weight = column_of(prob_ref[...], tok) * score / jnp.sum(score, axis=1, keepdims=True)
        lane = iota((tok, 128), 1)
        dense = jnp.zeros((tok, 128), F32)
        for k in range(member_ref.shape[1]):
            named = lax.rem(lane, 8) == member_ref[:, k : k + 1]
            dense = jnp.where(named, weight[:, k : k + 1], dense)
        parts = split3(dense)
        factors = split3(factor)
        packed = jnp.zeros((tok, 128), F32)
        for k in range(3):
            packed = jnp.where(lax.div(lane, 8) == k, parts[k], packed)
            packed = jnp.where(lane == 24 + k, factors[k], packed)
        meta_src[...] = dot(picker, packed.astype(BF16)).astype(BF16)
        for c, offsets in enumerate(CHUNKS):
            for j, offset in enumerate(offsets):
                place = pl.ds(j * cap, cap)
                if offset == 0:
                    meta[c, place, :] = meta_src[block_of(0), :]
                else:
                    send(meta_src.at[block_of(offset)], meta.at[c, place], z_send.at[1], m_recv.at[c], at_chip(-offset))

    def pass_meta(c):
        await_bytes(meta.at[c, remote_rows(c)], m_recv.at[c])
        send(meta.at[c, pl.ds(0, n_mine)], meta.at[c, pl.ds(n_mine, n_mine)], mfwd_send.at[c], mfwd_recv.at[c], partner)

    gate_cols, up_cols = pl.ds(0, cols), pl.ds(cols, cols)

    def partial(c, owner):
        return dot(rows[c], wgu[owner])

    def reduce_step(c, s):
        if s == 0:
            both = partial(c, x_index(half)).astype(BF16)
            rs_send[c, 0, 0, :, cols:] = both[:, cols:]
            rs_send[c, 0, 1, :, :cols] = both[:, :cols]
            send(rs_send.at[c, 0, 0, :, up_cols], rs_recv.at[c, 0, 0, :, up_cols], rs_ssem.at[c, 0, 0], rs_rsem.at[c, 0, 0], right)
            send(rs_send.at[c, 0, 1, :, gate_cols], rs_recv.at[c, 0, 1, :, gate_cols], rs_ssem.at[c, 0, 1], rs_rsem.at[c, 0, 1], left)
            return
        for d, (sign, device) in enumerate(((1, right), (-1, left))):
            mine = partial(c, x_index(sign * (half - s)))
            await_reduce(c, s - 1, d)
            if s == 1:
                lo, hi = (0, cols) if d == 0 else (cols, 2 * cols)
                alone = slice(lo, hi)
                other = slice(cols - lo, 2 * cols - lo)
                rs_send[c, s, d, :, alone] = mine[:, alone].astype(BF16)
                rs_send[c, s, d, :, other] = (mine[:, other] + rs_recv[c, s - 1, d, :, other].astype(F32)).astype(BF16)
            else:
                rs_send[c, s, d] = (mine + rs_recv[c, s - 1, d].astype(F32)).astype(BF16)
            send(rs_send.at[c, s, d], rs_recv.at[c, s, d], rs_ssem.at[c, s, d], rs_rsem.at[c, s, d], device)

    def reduce_ref(buf, c, s, d):
        if s > 0:
            return buf.at[c, s, d]
        return buf.at[c, s, d, :, up_cols if d == 0 else gate_cols]

    def await_reduce(c, s, d):
        await_bytes(reduce_ref(rs_recv, c, s, d), rs_rsem.at[c, s, d])

    def gather_ref(c, s, d, owner):
        if s < half - 1:
            return hid.at[c, owner]
        return hid.at[c, owner, pl.ds(d * n_mine, n_mine)]

    def gather_send(c, s):
        for d, (sign, device) in enumerate(((1, right), (-1, left))):
            block = gather_ref(c, s, d, x_index(-sign * s))
            send(block, block, ag_ssem.at[c, s, d], ag_rsem.at[c, s, d], device)

    def gather_wait(c, s):
        for d, sign in enumerate((1, -1)):
            await_bytes(gather_ref(c, s, d, x_index(-sign * (s + 1))), ag_rsem.at[c, s, d])

    def activate(c):
        total = partial(c, me)
        await_bytes(meta.at[c, pl.ds(n_mine, n_mine)], mfwd_recv.at[c])
        lane = iota((n_rows, 128), 1)
        info = meta[c].astype(F32)
        factor = jnp.sum(jnp.where(lax.div(lane, 8) == 3, info, 0.0), axis=1, keepdims=True)
        for d in range(2):
            await_reduce(c, half - 1, d)
            total = total + rs_recv[c, half - 1, d].astype(F32)
        total = total * factor
        gate, up = total[:, :cols], total[:, cols:]
        hid[c, me] = (gate / (1.0 + jnp.exp(-gate)) * up).astype(BF16)
        gather_send(c, 0)

    def produce(c):
        gather_wait(c, half - 1)
        hidden = jnp.concatenate([hid[c, o] for o in range(n_x)], axis=1)
        made = dot(hidden, wdn[...])
        lane = iota((n_rows, 128), 1)
        info = meta[c].astype(F32)
        member = 2 * lax.rem(z, per_chips) + core
        named = (lax.rem(lane, 8) == member) & (lane < 24)
        weight = jnp.sum(jnp.where(named, info, 0.0), axis=1, keepdims=True)
        made = made.astype(BF16).astype(F32) * weight
        pair_send[c] = made[n_mine:].astype(BF16)
        send(pair_send.at[c], pair_recv.at[c], pair_ssem.at[c], pair_rsem.at[c], partner)
        kept[c] = made[:n_mine]

    def give_back(c):
        await_bytes(pair_recv.at[c], pair_rsem.at[c])
        ret_send[c] = (kept[c] + pair_recv[c].astype(F32)).astype(BF16)
        for j, offset in enumerate(CHUNKS[c]):
            place = pl.ds(j * cap, cap)
            if offset == 0:
                ret_recv[c, place, :] = ret_send[c, place, :]
            else:
                send(ret_send.at[c, place], ret_recv.at[c, place], z_send.at[2], r_recv.at[c], at_chip(offset))

    def stage(c, k):
        if k == 0:
            await_bytes(rows.at[c, pl.ds(n_mine, n_mine)], fwd_recv.at[c])
            reduce_step(c, 0)
        elif k < half:
            reduce_step(c, k)
            if k == half - 2:
                pass_meta(c)
        elif k == half:
            activate(c)
        elif k < 2 * half:
            gather_wait(c, k - half - 1)
            gather_send(c, k - half)
        elif k == 2 * half:
            produce(c)
        else:
            give_back(c)

    last = 2 * half + 1
    n_chunks = len(CHUNKS)
    for t in range(max(START) + last + 1):
        for c in range(n_chunks):
            if t == max(START[c] - 1, 0) and (c == 0 or t > 0):
                take(c)
        if t == 0:
            await_bytes(wgu, w_sem.at[0])
        for c in range(n_chunks):
            k = t - START[c]
            if 0 <= k <= last:
                stage(c, k)
        if t == 0:
            send_meta()
            await_bytes(wdn, w_sem.at[1])

    moe = jnp.zeros((tok, dl), F32)
    for c, offsets in enumerate(CHUNKS):
        await_bytes(ret_recv.at[c, remote_rows(c)], r_recv.at[c])
        lane = iota((1, n_mine), 1)
        slots = lax.rem(lane, cap)
        for j, offset in enumerate(offsets):
            slots = slots + jnp.where(lax.div(lane, cap) == j, lax.div(chip(-offset), per_chips) * cap, 0)
        unpick = (jnp.broadcast_to(slot_col, (tok, n_mine)) == jnp.broadcast_to(slots.astype(F32), (tok, n_mine))).astype(BF16)
        moe = moe + dot(unpick, ret_recv[c])
    summed = tokens_ref[...].astype(F32) + moe
    square = jnp.sum(summed * summed, axis=1, keepdims=True)
    sq2_buf[pl.ds(me, 1)] = row_of(square, 128).reshape(1, 1, 128)
    for k in range(1, n_x):
        send(sq2_buf.at[me], sq2_buf.at[me], sq_send.at[1], sq_recv.at[1], peer(k))
    await_bytes(sq2_buf.at[pl.ds(0, n_x - 1)], sq_recv.at[1])
    total = column_of(jnp.sum(sq2_buf[...], axis=0), tok)
    out_ref[...] = (summed * lax.rsqrt(total / width + EPS) * final_ref[...]).astype(BF16)

    n_remote = cap * (n_z - 1)
    flat = wdn.at[pl.ds(0, n_remote)]
    await_bytes(flat, z_send.at[0])
    await_bytes(wdn.at[pl.ds(0, n_remote), pl.ds(0, 128)], z_send.at[1])
    await_bytes(flat, z_send.at[2])
    await_bytes(sq_buf.at[pl.ds(0, n_x - 1)], sq_send.at[0])
    await_bytes(sq_buf.at[pl.ds(0, n_x - 1)], sq_send.at[1])
    for c in range(n_chunks):
        await_bytes(rows.at[c, pl.ds(0, n_mine)], fwd_send.at[c])
        await_bytes(meta.at[c, pl.ds(0, n_mine)], mfwd_send.at[c])
        await_bytes(pair_recv.at[c], pair_ssem.at[c])
        for s in range(half):
            for d in range(2):
                await_bytes(reduce_ref(rs_send, c, s, d), rs_ssem.at[c, s, d])
                await_bytes(gather_ref(c, s, d, me), ag_ssem.at[c, s, d])


def local(tokens, group_choice, member_choice, group_prob, member_score, norm_gain, w_gate, w_up, w_down, final_gain):
    n_z, n_x = lax.axis_size("ep") // 2, lax.axis_size("tp")
    groups = max(2, 2 * n_z // 8)
    tok, dl = tokens.shape
    ff = w_gate.shape[2]
    cap = tok // groups
    cols = ff // n_x
    n_chunks = len(CHUNKS)
    n_mine = cap * len(CHUNKS[0])
    n_rows = 2 * n_mine
    half = n_x // 2
    dma = pltpu.SemaphoreType.DMA
    vmem = pl.BlockSpec(memory_space=pltpu.VMEM)
    hbm = pl.BlockSpec(memory_space=pl.ANY)
    return pl.pallas_call(
        functools.partial(kernel, (n_z, n_x, groups, dl * n_x)),
        out_shape=jax.ShapeDtypeStruct((tok, dl), BF16),
        in_specs=[vmem] * 7 + [hbm] * 3,
        out_specs=vmem,
        scratch_shapes=[
            pltpu.VMEM((n_x, dl, 2 * cols), BF16),
            pltpu.VMEM((ff, dl), BF16),
            pltpu.VMEM((tok, dl), BF16),
            pltpu.VMEM((tok, 128), BF16),
            pltpu.VMEM((n_chunks, n_rows, dl), BF16),
            pltpu.VMEM((n_chunks, n_rows, 128), BF16),
            pltpu.VMEM((n_x, 1, 128), F32),
            pltpu.VMEM((n_x, 1, 128), F32),
            pltpu.VMEM((n_chunks, half, 2, n_rows, 2 * cols), BF16),
            pltpu.VMEM((n_chunks, half, 2, n_rows, 2 * cols), BF16),
            pltpu.VMEM((n_chunks, n_x, n_rows, cols), BF16),
            pltpu.VMEM((n_chunks, n_mine, dl), F32),
            pltpu.VMEM((n_chunks, n_mine, dl), BF16),
            pltpu.VMEM((n_chunks, n_mine, dl), BF16),
            pltpu.VMEM((n_chunks, n_mine, dl), BF16),
            pltpu.VMEM((n_chunks, n_mine, dl), BF16),
            dma((2,)),
            dma((3,)),
            dma((n_chunks,)),
            dma((n_chunks,)),
            dma((n_chunks,)),
            dma((n_chunks,)),
            dma((n_chunks,)),
            dma((n_chunks,)),
            dma((2,)),
            dma((2,)),
            dma((n_chunks, half, 2)),
            dma((n_chunks, half, 2)),
            dma((n_chunks, half, 2)),
            dma((n_chunks, half, 2)),
            dma((n_chunks,)),
            dma((n_chunks,)),
            dma((n_chunks,)),
        ],
        compiler_params=pltpu.CompilerParams(
            collective_id=0, has_side_effects=True, vmem_limit_bytes=48 * 1024 * 1024
        ),
    )(
        tokens,
        group_choice.reshape(1, tok),
        member_choice,
        group_prob.reshape(1, tok),
        member_score,
        norm_gain.reshape(1, dl),
        final_gain.reshape(1, dl),
        w_gate,
        w_up,
        w_down,
    )


def solution(mesh):
    rows = ("grp", "ep")
    placed = (
        P(rows, "tp"),
        P(rows),
        P(rows, None),
        P(rows),
        P(rows, None),
        P("tp"),
        P("ep", "tp", None),
        P("ep", "tp", None),
        P("ep", None, "tp"),
        P("tp"),
    )
    return jax.shard_map(local, mesh=mesh, in_specs=placed, out_specs=P(rows, "tp"), check_vma=False)
```

time: 240 us -> 134 us (0.56)
  Pallas kernels: 0 us -> 126 us
  blocking collectives: 121 us -> 0 us
  waiting for transfers between devices: 69.1 us -> 0 us
  starting transfers between devices: 20.7 us -> 0 us
  between operations: 13.6 us -> 0.07 us
  other arithmetic: 4.83 us -> 0 us
  matrix products: 3.69 us -> 0 us
    pallas_call x0 -> x1, Pallas kernels: none -> 126 us  [local(): pl.pallas_call(functools.partial(kernel, (n_z, n_x, groups, dl * n_x)), o...]
    all_to_all x4 -> x0, blocking collectives: 121 us -> none  [the longest x1 77.3 us: local(): lax.all_to_all(outgoing, EP, split_axis=0, concat_axis=0, tiled=True)]
    reduce_scatter x1 -> x0, waiting for transfers between devices: 35.6 us -> none  [sum_together(): lax.psum_scatter(lines, axis, tiled=True).reshape(-1)]
    all_to_all x2 -> x0, waiting for transfers between devices: 33.5 us -> none  [the longest x1 29 us: turned_blocks(): whole = lax.all_to_all(whole, axes[k], k, k, tiled=True)]
    all_to_all x2 -> x0, starting transfers between devices: 20.6 us -> none  [the longest x1 13.3 us: turned_blocks(): whole = lax.all_to_all(whole, axes[k], k, k, tiled=True)]
    unnamed x17 -> x19, local copies, waits for them, and re-layouts: 1.57 us -> 5.92 us
    dot_general x5 -> x0, matrix products: 3.69 us -> none  [the longest x1 1.18 us: local(): jnp.einsum('tkr,td->rd', picker, normed, preferred_element_type=jnp.float32)]
  transfers between devices with their start and end apart: 3 -> 0, of which waited for: 3 -> 0; matrix products, arithmetic and copies ran while one was open for 1% -> 0% of each run, Pallas kernels for 0% -> 0%
where the time goes in v1:
time: 134 us; the launch traced here: 132 us
  Pallas kernels  126 us (94%)
  local copies, waits for them, and re-layouts  5.92 us (4%)
    pallas_call x1, Pallas kernels, local(): pl.pallas_call(functools.partial(kernel, (n_z, n_x, groups, dl * n_x)), o...  126 us
    unnamed x19, local copies, waits for them, and re-layouts  5.92 us

profile of v1, /device:TPU:80, one launch (start us, length us, event | category | flops | bytes accessed | tf_op | source)
XLA Modules:
  0.0 132.5 jit_solution(6299758671213417757)
XLA Ops:
  0.0 0.0 copy-start.3
  0.0 0.8 copy.11.member_ref
  0.8 0.0 copy-start.4
  0.8 0.0 copy-start.5
  0.8 0.0 copy-start.6
  0.8 0.0 copy-start.7
  0.8 0.8 copy.12.score_ref
  1.6 0.0 copy-done.3
  1.6 0.0 copy-done.4
  1.6 0.0 copy-done.5
  1.7 0.0 copy-done.6
  1.7 0.0 copy-done.7
  1.7 0.0 copy-start
  1.7 1.2 copy-done
  2.9 0.0 copy-start.1
  2.9 1.2 copy-done.1
  4.1 0.0 copy-start.2
  4.1 1.2 copy-done.2
  5.4 126.5 %shard_map.100 = bf16[64,512]{1,0:T(8,128)(2,1)S(1)} custom-call(bf16[64,512]{1,0:T(8,128)(2,1)S(1)} %copy-done.3, s32[1,64]{1,0:T(1,128)S(1)} %bitcast.6, s32[64,4]{1,0:T(8,128)S(1)} %copy.11.member_ref, f32[1,64]{1,0:T(1,128)S(1)} %bitcast.7, f32[64,4]{1,0:T(8,128)S(1)} %copy.12.score_ref, f32[1,512]{1,0:T(1,128)S(1)} %bitcast.4, f32[1,512]{1,0:T(1,128)S(1)} %bitcast.5, ...), custom_call_target="tpu_custom_call" | custom-call | tf_op jit(solution)/shard_map/pallas_call | solution.py:377
  131.8 0.6 copy.14
Async XLA Ops:
  0.0 1.6 %copy-start.3 = (bf16[64,512]{1,0:T(8,128)(2,1)S(1)}, bf16[64,512]{1,0:T(8,128)(2,1)}, u32[]{:S(2)}) copy-start(bf16[64,512]{1,0:T(8,128)(2,1)} %tokens_ref.1) | copy-start | bytes 196612
  0.8 0.8 copy-start.4
  0.8 0.8 copy-start.5
  0.8 0.8 copy-start.6
  0.8 0.8 copy-start.7
  1.7 1.2 copy-start
  2.9 1.2 copy-start.1
  4.1 1.2 copy-start.2

commit v2 on v1

v2 whole, which is shorter than its diff:
```python
import functools

import jax
import jax.numpy as jnp
from jax import lax
from jax.experimental import pallas as pl
from jax.experimental.pallas import tpu as pltpu
from jax.sharding import PartitionSpec as P

EPS = 1e-06
F32 = jnp.float32
BF16 = jnp.bfloat16
MESH = pl.DeviceIdType.MESH

CHUNKS = (4, 4, 4, 4)
START = (0, 1, 2, 3)


def dot(a, b):
    return jnp.dot(a, b, preferred_element_type=F32)


def iota(shape, dim):
    return lax.broadcasted_iota(jnp.int32, shape, dim)


def column_of(row, n):
    shape = (n, row.shape[1])
    same = iota(shape, 0) == iota(shape, 1)
    return jnp.sum(jnp.where(same, jnp.broadcast_to(row, shape), 0.0), axis=1, keepdims=True)


def row_of(column, lanes):
    shape = (column.shape[0], lanes)
    same = iota(shape, 0) == iota(shape, 1)
    return jnp.sum(jnp.where(same, jnp.broadcast_to(column, shape), 0.0), axis=0, keepdims=True)


def split3(value):
    first = value.astype(BF16).astype(F32)
    rest = value - first
    second = rest.astype(BF16).astype(F32)
    third = (rest - second).astype(BF16).astype(F32)
    return first, second, third


def kernel(
    dims,
    tokens_ref,
    group_ref,
    member_ref,
    prob_ref,
    score_ref,
    gain_ref,
    final_ref,
    wg_ref,
    wu_ref,
    wd_ref,
    out_ref,
    wgu,
    wdn,
    sorted_buf,
    meta_src,
    rows_mine,
    rows_other,
    meta_mine,
    meta_other,
    sq_buf,
    sq2_buf,
    rs_send,
    rs_recv,
    hid,
    kept,
    pair_send,
    pair_recv,
    ret_send,
    ret_recv,
    summed_buf,
    w_sem,
    z_send,
    z_recv,
    m_recv,
    r_recv,
    fwd_send,
    fwd_recv,
    mfwd_send,
    mfwd_recv,
    sq_send,
    sq_recv,
    rs_ssem,
    rs_rsem,
    ag_ssem,
    ag_rsem,
    pair_ssem,
    pair_rsem,
    here_z,
    here_x,
    here_c,
):
    n_z, n_x, groups, width = dims
    per_chips = n_z // groups
    tok, dl = tokens_ref.shape
    cap = tok // groups
    half = n_x // 2
    cols = wgu.shape[2] // 2
    n_chunks = len(CHUNKS)
    bases = [sum(CHUNKS[:c]) for c in range(n_chunks)]
    ep, me = lax.axis_index("ep"), lax.axis_index("tp")
    z, core = lax.div(ep, 2), lax.rem(ep, 2)
    partner = {"ep": 2 * z + 1 - core}
    right = {"tp": lax.rem(me + 1, n_x)}
    left = {"tp": lax.rem(me + n_x - 1, n_x)}

    def at_chip(k):
        return {"ep": 2 * k + core}

    def x_index(offset):
        return lax.rem(me + offset + n_x, n_x)

    def block(index):
        return pl.ds(pl.multiple_of(index * cap, cap), cap)

    def span(c):
        return pl.ds(bases[c] * cap, CHUNKS[c] * cap)

    def n_mine(c):
        return CHUNKS[c] * cap

    def in_chunk(c):
        return (z >= bases[c]) & (z < bases[c] + CHUNKS[c])

    def send(src, dst, ssem, rsem, device):
        pltpu.make_async_remote_copy(
            src_ref=src, dst_ref=dst, send_sem=ssem, recv_sem=rsem, device_id=device, device_id_type=MESH
        ).start()

    def await_bytes(ref, sem):
        pltpu.make_async_copy(ref, ref, sem).wait()

    def signal(sem, device):
        pl.semaphore_signal(sem, inc=1, device_id=device, device_id_type=MESH)

    def each(lo, hi, body):
        def step(i, carry):
            body(i)
            return carry

        lax.fori_loop(lo, hi, step, 0)

    def ranked(index, n, odd):
        moved = jnp.where(index == 0, n - 2, jnp.where(index == n - 1, n - 1, index - 1))
        return jnp.where(odd, moved, index)

    def unranked(rank, n, odd):
        moved = jnp.where(rank == n - 2, 0, jnp.where(rank == n - 1, n - 1, rank + 1))
        return jnp.where(odd, moved, rank)

    def folded(index):
        return jnp.where(index < half, index, n_x - 1 - index + half)

    z_odd, x_odd, c_odd = (me == 0) & (core == 0), (z == 0) & (core == 0), (z == 0) & (me == 0)
    z_rank = ranked(z, n_z, z_odd)
    x_rank = jnp.where(x_odd, lax.rem(folded(me) + n_x - 1, n_x), folded(me))
    c_rank = jnp.where(c_odd, 1 - core, core)

    def z_of(rank):
        return unranked(rank, n_z, z_odd)

    def x_of(rank):
        return folded(jnp.where(x_odd, lax.rem(rank + 1, n_x), rank))

    barrier = pltpu.get_barrier_semaphore()
    each(z_rank + 1, n_z, lambda r: signal(barrier, at_chip(z_of(r))))
    each(x_rank + 1, n_x, lambda r: signal(barrier, {"tp": x_of(r)}))

    @pl.when(c_rank == 0)
    def _():
        signal(barrier, partner)

    loads = []
    for o in range(n_x):
        part = pl.ds(o * cols, cols)
        loads.append(pltpu.make_async_copy(wg_ref.at[0, :, part], wgu.at[o, :, pl.ds(0, cols)], w_sem.at[0]))
        loads.append(pltpu.make_async_copy(wu_ref.at[0, :, part], wgu.at[o, :, pl.ds(cols, cols)], w_sem.at[0]))
    loads.append(pltpu.make_async_copy(wd_ref.at[0], wdn, w_sem.at[1]))
    for load in loads:
        load.start()

    values = tokens_ref[...].astype(F32)
    scaled = (values * gain_ref[...]).astype(BF16)
    group_row = group_ref[...]
    chosen = (iota((8, tok), 0) == jnp.broadcast_to(group_row, (8, tok))).astype(F32)
    earlier = (iota((tok, tok), 0) < iota((tok, tok), 1)).astype(F32)
    rank = jnp.sum(dot(chosen, earlier) * chosen, axis=0, keepdims=True)
    slot_row = group_row.astype(F32) * cap + rank
    picker = (iota((tok, tok), 0).astype(F32) == jnp.broadcast_to(slot_row, (tok, tok))).astype(BF16)
    sorted_buf[...] = dot(picker, scaled).astype(BF16)
    square = jnp.sum(values * values, axis=1, keepdims=True)
    sq_buf[pl.ds(me, 1)] = row_of(square, 128).reshape(1, 1, 128)
    rows_mine[block(z), :] = sorted_buf[block(lax.div(z, per_chips)), :]

    def send_rows(k):
        send(sorted_buf.at[block(lax.div(k, per_chips))], rows_mine.at[block(z)], z_send.at[0], z_recv.at[z], at_chip(k))

    def send_meta(k):
        send(meta_src.at[block(lax.div(k, per_chips))], meta_mine.at[block(z)], z_send.at[1], m_recv.at[z], at_chip(k))

    with jax.named_scope("meet"):
        expected = z_rank + x_rank + c_rank

        @pl.when(expected > 0)
        def _():
            pl.semaphore_wait(barrier, expected)

        each(0, z_rank, lambda r: signal(here_z.at[z], at_chip(z_of(r))))
        each(0, x_rank, lambda r: signal(here_x.at[me], {"tp": x_of(r)}))

        @pl.when(c_rank == 1)
        def _():
            signal(here_c, partner)

    def greet(r):
        k = z_of(r)
        pl.semaphore_wait(here_z.at[k], 1)
        send_rows(k)

    with jax.named_scope("greet"):
        each(0, z_rank, lambda r: send_rows(z_of(r)))
        each(z_rank + 1, n_z, greet)

    def send_square(r):
        send(sq_buf.at[me], sq_buf.at[me], sq_send.at[0], sq_recv.at[0], {"tp": x_of(r)})

    def greet_x(r):
        pl.semaphore_wait(here_x.at[x_of(r)], 1)
        send_square(r)

    with jax.named_scope("greet_x"):
        each(0, x_rank, send_square)
        each(x_rank + 1, n_x, greet_x)

        @pl.when(c_rank == 0)
        def _():
            pl.semaphore_wait(here_c, 1)

    def await_blocks(c, ref, sems):
        for k in range(bases[c], bases[c] + CHUNKS[c]):

            @pl.when(z != k)
            def _(k=k):
                await_bytes(ref.at[pl.ds(k * cap, cap)], sems.at[k])

    def take(c):
        await_blocks(c, rows_mine, z_recv)
        send(rows_mine.at[span(c)], rows_other.at[span(c)], fwd_send.at[c], fwd_recv.at[c], partner)

    def make_meta():
        await_bytes(sq_buf.at[pl.ds(0, n_x - 1)], sq_recv.at[0])
        total = jnp.sum(sq_buf[...], axis=0)[:, :tok]
        factor = lax.rsqrt(total / width + EPS)
        score = jnp.exp(score_ref[...])
        weight = prob_ref[...] * score / jnp.sum(score, axis=0, keepdims=True)
        member = iota((8, tok), 0)
        dense = jnp.zeros((8, tok), F32)
        for k in range(member_ref.shape[0]):
            dense = jnp.where(member == member_ref[k : k + 1, :], weight[k : k + 1, :], dense)
        parts = split3(dense)
        factors = split3(factor)
        spread = jnp.zeros((8, tok), F32)
        for k in range(3):
            spread = jnp.where(member == k, factors[k], spread)
        packed = jnp.concatenate([*parts, spread, jnp.zeros((96, tok), F32)], axis=0)
        meta_src[...] = lax.dot_general(
            picker, packed.astype(BF16), (((1,), (1,)), ((), ())), preferred_element_type=F32
        ).astype(BF16)
        meta_mine[block(z), :] = meta_src[block(lax.div(z, per_chips)), :]
        each(0, z_rank, lambda r: send_meta(z_of(r)))
        each(z_rank + 1, n_z, lambda r: send_meta(z_of(r)))

    def pass_meta(c):
        await_blocks(c, meta_mine, m_recv)
        send(meta_mine.at[span(c)], meta_other.at[span(c)], mfwd_send.at[c], mfwd_recv.at[c], partner)

    gate_cols, up_cols = pl.ds(0, cols), pl.ds(cols, cols)

    def partial(c, owner):
        both = jnp.concatenate([rows_mine[span(c), :], rows_other[span(c), :]], axis=0)
        return dot(both, wgu[owner])

    def reduce_ref(buf, c, s, d):
        used = pl.ds(0, 2 * n_mine(c))
        if s > 0:
            return buf.at[c, s, d, used]
        return buf.at[c, s, d, used, up_cols if d == 0 else gate_cols]

    def await_reduce(c, s, d):
        await_bytes(reduce_ref(rs_recv, c, s, d), rs_rsem.at[c, s, d])

    def reduce_send(c, s, d):
        send(
            reduce_ref(rs_send, c, s, d),
            reduce_ref(rs_recv, c, s, d),
            rs_ssem.at[c, s, d],
            rs_rsem.at[c, s, d],
            right if d == 0 else left,
        )

    def reduce_step(c, s):
        n = 2 * n_mine(c)
        if s == 0:
            both = partial(c, x_index(half)).astype(BF16)
            rs_send[c, 0, 0, :n, cols:] = both[:, cols:]
            rs_send[c, 0, 1, :n, :cols] = both[:, :cols]
            reduce_send(c, 0, 0)
            reduce_send(c, 0, 1)
            return
        for d, sign in enumerate((1, -1)):
            mine = partial(c, x_index(sign * (half - s)))
            await_reduce(c, s - 1, d)
            if s == 1:
                lo = d * cols
                alone = slice(lo, lo + cols)
                other = slice(cols - lo, 2 * cols - lo)
                rs_send[c, s, d, :n, alone] = mine[:, alone].astype(BF16)
                rs_send[c, s, d, :n, other] = (mine[:, other] + rs_recv[c, s - 1, d, :n, other].astype(F32)).astype(BF16)
            else:
                rs_send[c, s, d, :n] = (mine + rs_recv[c, s - 1, d, :n].astype(F32)).astype(BF16)
            reduce_send(c, s, d)

    def gather_ref(c, s, d, owner):
        if s < half - 1:
            return hid.at[c, owner, pl.ds(0, 2 * n_mine(c))]
        return hid.at[c, owner, pl.ds(d * n_mine(c), n_mine(c))]

    def gather_send(c, s):
        for d, sign in enumerate((1, -1)):
            ref = gather_ref(c, s, d, x_index(-sign * s))
            send(ref, ref, ag_ssem.at[c, s, d], ag_rsem.at[c, s, d], right if d == 0 else left)

    def gather_wait(c, s):
        for d, sign in enumerate((1, -1)):
            await_bytes(gather_ref(c, s, d, x_index(-sign * (s + 1))), ag_rsem.at[c, s, d])

    def info(c):
        return jnp.concatenate([meta_mine[span(c), :], meta_other[span(c), :]], axis=0).astype(F32)

    def activate(c):
        n = 2 * n_mine(c)
        total = partial(c, me)
        await_bytes(meta_other.at[span(c)], mfwd_recv.at[c])
        lane = iota((n, 128), 1)
        factor = jnp.sum(jnp.where(lax.div(lane, 8) == 3, info(c), 0.0), axis=1, keepdims=True)
        for d in range(2):
            await_reduce(c, half - 1, d)
            total = total + rs_recv[c, half - 1, d, :n].astype(F32)
        total = total * factor
        gate, up = total[:, :cols], total[:, cols:]
        hid[c, me, :n] = (gate / (1.0 + jnp.exp(-gate)) * up).astype(BF16)
        gather_send(c, 0)

    def produce(c):
        n = 2 * n_mine(c)
        gather_wait(c, half - 1)
        hidden = jnp.concatenate([hid[c, o, :n] for o in range(n_x)], axis=1)
        made = dot(hidden, wdn[...])
        lane = iota((n, 128), 1)
        member = 2 * lax.rem(z, per_chips) + core
        named = (lax.rem(lane, 8) == member) & (lane < 24)
        weight = jnp.sum(jnp.where(named, info(c), 0.0), axis=1, keepdims=True)
        made = made.astype(BF16).astype(F32) * weight
        pair_send[span(c), :] = made[n_mine(c) :].astype(BF16)
        send(pair_send.at[span(c)], pair_recv.at[span(c)], pair_ssem.at[c], pair_rsem.at[c], partner)
        kept[span(c), :] = made[: n_mine(c)]

    def give_back(c):
        await_bytes(pair_recv.at[span(c)], pair_rsem.at[c])
        ret_send[span(c), :] = (kept[span(c), :] + pair_recv[span(c), :].astype(F32)).astype(BF16)
        for k in range(bases[c], bases[c] + CHUNKS[c]):

            @pl.when(z == k)
            def _(k=k):
                ret_recv[block(k), :] = ret_send[block(k), :]

            @pl.when(z != k)
            def _(k=k):
                send(ret_send.at[block(k)], ret_recv.at[block(z)], z_send.at[2], r_recv.at[z], at_chip(k))

    def gather_returned():
        for k in range(n_z):

            @pl.when(z != k)
            def _(k=k):
                await_bytes(ret_recv.at[block(k)], r_recv.at[k])

        row = iota((n_z * cap, tok), 0)
        slots = lax.div(row, per_chips * cap) * cap + lax.rem(row, cap)
        unpick = (slots.astype(F32) == jnp.broadcast_to(slot_row, row.shape)).astype(BF16)
        moe = lax.dot_general(unpick, ret_recv[...], (((0,), (0,)), ((), ())), preferred_element_type=F32)
        summed = tokens_ref[...].astype(F32) + moe
        summed_buf[...] = summed
        total = jnp.sum(summed * summed, axis=1, keepdims=True)
        sq2_buf[pl.ds(me, 1)] = row_of(total, 128).reshape(1, 1, 128)

        def send_total(r):
            send(sq2_buf.at[me], sq2_buf.at[me], sq_send.at[1], sq_recv.at[1], {"tp": r})

        each(0, me, send_total)
        each(me + 1, n_x, send_total)

    def write_out():
        await_bytes(sq2_buf.at[pl.ds(0, n_x - 1)], sq_recv.at[1])
        total = column_of(jnp.sum(sq2_buf[...], axis=0), tok)
        out_ref[...] = (summed_buf[...] * lax.rsqrt(total / width + EPS) * final_ref[...]).astype(BF16)

    def stage(c, k):
        if k == 0:
            await_bytes(rows_other.at[span(c)], fwd_recv.at[c])
            reduce_step(c, 0)
        elif k < half:
            reduce_step(c, k)
            if k == half - 2:
                pass_meta(c)
        elif k == half:
            activate(c)
        elif k < 2 * half:
            gather_wait(c, k - half - 1)
            gather_send(c, k - half)
        elif k == 2 * half:
            produce(c)
        else:
            give_back(c)

    last = 2 * half + 1
    with jax.named_scope("take#c=0"):
        take(0)
    with jax.named_scope("weights"):
        await_bytes(wgu, w_sem.at[0])
        await_bytes(wdn, w_sem.at[1])
    for t in range(START[-1] + last + 1):
        for c in range(n_chunks):
            k = t - START[c]
            if 0 <= k <= last:
                with jax.named_scope(f"stage#c={c}#k={k}"):
                    stage(c, k)
            if k == -1:
                with jax.named_scope(f"take#c={c}"):
                    take(c)
        if t == 1:
            with jax.named_scope("make_meta"):
                make_meta()
    with jax.named_scope("returned"):
        gather_returned()
    with jax.named_scope("write"):
        write_out()

    n_remote = cap * (n_z - 1)
    flat = wdn.at[pl.ds(0, n_remote)]
    await_bytes(flat, z_send.at[0])
    await_bytes(wdn.at[pl.ds(0, n_remote), pl.ds(0, 128)], z_send.at[1])
    await_bytes(flat, z_send.at[2])
    await_bytes(sq_buf.at[pl.ds(0, n_x - 1)], sq_send.at[0])
    await_bytes(sq_buf.at[pl.ds(0, n_x - 1)], sq_send.at[1])
    for c in range(n_chunks):
        await_bytes(rows_mine.at[span(c)], fwd_send.at[c])
        await_bytes(meta_mine.at[span(c)], mfwd_send.at[c])
        await_bytes(pair_recv.at[span(c)], pair_ssem.at[c])
        for s in range(half):
            for d in range(2):
                await_bytes(reduce_ref(rs_send, c, s, d), rs_ssem.at[c, s, d])
                await_bytes(gather_ref(c, s, d, me), ag_ssem.at[c, s, d])


def local(tokens, group_choice, member_choice, group_prob, member_score, norm_gain, w_gate, w_up, w_down, final_gain):
    n_z, n_x = lax.axis_size("ep") // 2, lax.axis_size("tp")
    groups = max(2, 2 * n_z // 8)
    tok, dl = tokens.shape
    ff = w_gate.shape[2]
    cap = tok // groups
    cols = ff // n_x
    n_chunks = len(CHUNKS)
    n_rows = 2 * cap * max(CHUNKS)
    n_all = n_z * cap
    half = n_x // 2
    dma = pltpu.SemaphoreType.DMA
    vmem = pl.BlockSpec(memory_space=pltpu.VMEM)
    hbm = pl.BlockSpec(memory_space=pl.ANY)
    return pl.pallas_call(
        functools.partial(kernel, (n_z, n_x, groups, dl * n_x)),
        out_shape=jax.ShapeDtypeStruct((tok, dl), BF16),
        in_specs=[vmem] * 7 + [hbm] * 3,
        out_specs=vmem,
        scratch_shapes=[
            pltpu.VMEM((n_x, dl, 2 * cols), BF16),
            pltpu.VMEM((ff, dl), BF16),
            pltpu.VMEM((tok, dl), BF16),
            pltpu.VMEM((tok, 128), BF16),
            pltpu.VMEM((n_all, dl), BF16),
            pltpu.VMEM((n_all, dl), BF16),
            pltpu.VMEM((n_all, 128), BF16),
            pltpu.VMEM((n_all, 128), BF16),
            pltpu.VMEM((n_x, 1, 128), F32),
            pltpu.VMEM((n_x, 1, 128), F32),
            pltpu.VMEM((n_chunks, half, 2, n_rows, 2 * cols), BF16),
            pltpu.VMEM((n_chunks, half, 2, n_rows, 2 * cols), BF16),
            pltpu.VMEM((n_chunks, n_x, n_rows, cols), BF16),
            pltpu.VMEM((n_all, dl), F32),
            pltpu.VMEM((n_all, dl), BF16),
            pltpu.VMEM((n_all, dl), BF16),
            pltpu.VMEM((n_all, dl), BF16),
            pltpu.VMEM((n_all, dl), BF16),
            pltpu.VMEM((tok, dl), F32),
            dma((2,)),
            dma((3,)),
            dma((n_z,)),
            dma((n_z,)),
            dma((n_z,)),
            dma((n_chunks,)),
            dma((n_chunks,)),
            dma((n_chunks,)),
            dma((n_chunks,)),
            dma((2,)),
            dma((2,)),
            dma((n_chunks, half, 2)),
            dma((n_chunks, half, 2)),
            dma((n_chunks, half, 2)),
            dma((n_chunks, half, 2)),
            dma((n_chunks,)),
            dma((n_chunks,)),
            pltpu.SemaphoreType.REGULAR((n_z,)),
            pltpu.SemaphoreType.REGULAR((n_x,)),
            pltpu.SemaphoreType.REGULAR,
        ],
        compiler_params=pltpu.CompilerParams(
            collective_id=0, has_side_effects=True, vmem_limit_bytes=67043328
        ),
    )(
        tokens,
        group_choice.reshape(1, tok),
        member_choice.T,
        group_prob.reshape(1, tok),
        member_score.T,
        norm_gain.reshape(1, dl),
        final_gain.reshape(1, dl),
        w_gate,
        w_up,
        w_down,
    )


def solution(mesh):
    rows = ("grp", "ep")
    placed = (
        P(rows, "tp"),
        P(rows),
        P(rows, None),
        P(rows),
        P(rows, None),
        P("tp"),
        P("ep", "tp", None),
        P("ep", "tp", None),
        P("ep", None, "tp"),
        P("tp"),
    )
    return jax.shard_map(local, mesh=mesh, in_specs=placed, out_specs=P(rows, "tp"), check_vma=False)
```

time: 134 us -> 112 us (0.84)
  Pallas kernels: 126 us -> 109 us
  local copies, waits for them, and re-layouts: 5.92 us -> 1.47 us
    pallas_call x1, Pallas kernels: 126 us -> 109 us  [local(): pl.pallas_call(functools.partial(kernel, (n_z, n_x, groups, dl * n_x)), o...]
    unnamed x19 -> x1, local copies, waits for them, and re-layouts: 5.92 us -> 1.47 us
where the time goes in v2:
time: 112 us; the launch traced here: 110 us
  Pallas kernels  109 us (97%)
  local copies, waits for them, and re-layouts  1.47 us (1%)
    pallas_call x1, Pallas kernels, local(): pl.pallas_call(functools.partial(kernel, (n_z, n_x, groups, dl * n_x)), o...  109 us

profile of v2, /device:TPU:80, one launch (start us, length us, event | category | flops | bytes accessed | tf_op | source)
XLA Modules:
  0.0 110.4 jit_solution(17916753288934745894)
XLA Ops:
  0.0 108.9 %shard_map.100 = bf16[64,512]{1,0:T(8,128)(2,1)} custom-call(bf16[64,512]{1,0:T(8,128)(2,1)} %tokens_ref.1, s32[1,64]{1,0:T(1,128)} %bitcast.10, s32[4,64]{1,0:T(4,128)} %bitcast.6, f32[1,64]{1,0:T(1,128)} %bitcast.11, f32[4,64]{1,0:T(4,128)} %bitcast.7, f32[1,512]{1,0:T(1,128)} %bitcast.8, f32[1,512]{1,0:T(1,128)} %bitcast.9, bf16[1,512,1024]{2,1,0:T(8,128)(2,1)} %wg_ref.1, ...), custom_call_target="tpu_custom_call" | custom-call | tf_op jit(solution)/shard_map/pallas_call | solution.py:487
  108.9 1.5 %copy.12 = bf16[64,512]{1,0:T(8,128)(2,1)} copy(bf16[64,512]{1,0:T(8,128)(2,1)} %shard_map.100) | data formatting | bytes 131072

commit v3 on v2

--- a/solution.py
+++ b/solution.py
@@ -13,7 +13,8 @@
 MESH = pl.DeviceIdType.MESH
 
 CHUNKS = (4, 4, 4, 4)
-START = (0, 1, 2, 3)
+START = (0, 1, 1, 1)
+DIRECT = ()
 
 
 def dot(a, b):
@@ -46,6 +47,17 @@
 
 def kernel(
     dims,
+    tokens_hbm,
+    group_hbm,
+    member_hbm,
+    prob_hbm,
+    score_hbm,
+    gain_hbm,
+    final_hbm,
+    wg_ref,
+    wu_ref,
+    wd_ref,
+    out_ref,
     tokens_ref,
     group_ref,
     member_ref,
@@ -53,10 +65,7 @@
     score_ref,
     gain_ref,
     final_ref,
-    wg_ref,
-    wu_ref,
-    wd_ref,
-    out_ref,
+    in_sem,
     wgu,
     wdn,
     sorted_buf,
@@ -99,7 +108,7 @@
 ):
     n_z, n_x, groups, width = dims
     per_chips = n_z // groups
-    tok, dl = tokens_ref.shape
+    tok, dl = tokens_hbm.shape
     cap = tok // groups
     half = n_x // 2
     cols = wgu.shape[2] // 2
@@ -177,6 +186,18 @@
     def _():
         signal(barrier, partner)
 
+    smalls = (
+        (tokens_hbm, tokens_ref),
+        (group_hbm, group_ref),
+        (gain_hbm, gain_ref),
+        (member_hbm, member_ref),
+        (prob_hbm, prob_ref),
+        (score_hbm, score_ref),
+        (final_hbm, final_ref),
+    )
+    fetched = [pltpu.make_async_copy(src, dst, in_sem.at[i]) for i, (src, dst) in enumerate(smalls)]
+    for fetch in fetched:
+        fetch.start()
     loads = []
     for o in range(n_x):
         part = pl.ds(o * cols, cols)
@@ -186,6 +207,8 @@
     for load in loads:
         load.start()
 
+    for fetch in fetched:
+        fetch.wait()
     values = tokens_ref[...].astype(F32)
     scaled = (values * gain_ref[...]).astype(BF16)
     group_row = group_ref[...]
@@ -332,6 +355,11 @@
             return hid.at[c, owner, pl.ds(0, 2 * n_mine(c))]
         return hid.at[c, owner, pl.ds(d * n_mine(c), n_mine(c))]
 
+    def gather_all(c):
+        for r in range(1, n_x):
+            block_me = hid.at[c, me, pl.ds(0, 2 * n_mine(c))]
+            send(block_me, block_me, ag_ssem.at[c, 0, 0], ag_rsem.at[c, 0, 0], {"tp": x_index(r)})
+
     def gather_send(c, s):
         for d, sign in enumerate((1, -1)):
             ref = gather_ref(c, s, d, x_index(-sign * s))
@@ -356,11 +384,20 @@
         total = total * factor
         gate, up = total[:, :cols], total[:, cols:]
         hid[c, me, :n] = (gate / (1.0 + jnp.exp(-gate)) * up).astype(BF16)
-        gather_send(c, 0)
+        if c in DIRECT:
+            gather_all(c)
+        else:
+            gather_send(c, 0)
+
+    def all_others(c):
+        return hid.at[c, pl.ds(0, n_x - 1), pl.ds(0, 2 * n_mine(c))]
 
     def produce(c):
         n = 2 * n_mine(c)
-        gather_wait(c, half - 1)
+        if c in DIRECT:
+            await_bytes(all_others(c), ag_rsem.at[c, 0, 0])
+        else:
+            gather_wait(c, half - 1)
         hidden = jnp.concatenate([hid[c, o, :n] for o in range(n_x)], axis=1)
         made = dot(hidden, wdn[...])
         lane = iota((n, 128), 1)
@@ -422,6 +459,8 @@
                 pass_meta(c)
         elif k == half:
             activate(c)
+        elif c in DIRECT:
+            (produce if k == half + 1 else give_back)(c)
         elif k < 2 * half:
             gather_wait(c, k - half - 1)
             gather_send(c, k - half)
@@ -430,16 +469,19 @@
         else:
             give_back(c)
 
-    last = 2 * half + 1
-    with jax.named_scope("take#c=0"):
-        take(0)
+    ends = [half + 2 if c in DIRECT else 2 * half + 1 for c in range(n_chunks)]
+    total_steps = max(START[c] + ends[c] for c in range(n_chunks)) + 1
+    for c in range(n_chunks):
+        if START[c] == 0:
+            with jax.named_scope(f"take#c={c}"):
+                take(c)
     with jax.named_scope("weights"):
         await_bytes(wgu, w_sem.at[0])
         await_bytes(wdn, w_sem.at[1])
-    for t in range(START[-1] + last + 1):
+    for t in range(total_steps):
         for c in range(n_chunks):
             k = t - START[c]
-            if 0 <= k <= last:
+            if 0 <= k <= ends[c]:
                 with jax.named_scope(f"stage#c={c}#k={k}"):
                     stage(c, k)
             if k == -1:
@@ -464,16 +506,20 @@
         await_bytes(rows_mine.at[span(c)], fwd_send.at[c])
         await_bytes(meta_mine.at[span(c)], mfwd_send.at[c])
         await_bytes(pair_recv.at[span(c)], pair_ssem.at[c])
+        if c in DIRECT:
+            await_bytes(all_others(c), ag_ssem.at[c, 0, 0])
         for s in range(half):
             for d in range(2):
                 await_bytes(reduce_ref(rs_send, c, s, d), rs_ssem.at[c, s, d])
-                await_bytes(gather_ref(c, s, d, me), ag_ssem.at[c, s, d])
+                if c not in DIRECT:
+                    await_bytes(gather_ref(c, s, d, me), ag_ssem.at[c, s, d])
 
 
 def local(tokens, group_choice, member_choice, group_prob, member_score, norm_gain, w_gate, w_up, w_down, final_gain):
     n_z, n_x = lax.axis_size("ep") // 2, lax.axis_size("tp")
     groups = max(2, 2 * n_z // 8)
     tok, dl = tokens.shape
+    top = member_choice.shape[1]
     ff = w_gate.shape[2]
     cap = tok // groups
     cols = ff // n_x
@@ -487,9 +533,17 @@
     return pl.pallas_call(
         functools.partial(kernel, (n_z, n_x, groups, dl * n_x)),
         out_shape=jax.ShapeDtypeStruct((tok, dl), BF16),
-        in_specs=[vmem] * 7 + [hbm] * 3,
+        in_specs=[hbm] * 10,
         out_specs=vmem,
         scratch_shapes=[
+            pltpu.VMEM((tok, dl), BF16),
+            pltpu.VMEM((1, tok), jnp.int32),
+            pltpu.VMEM((top, tok), jnp.int32),
+            pltpu.VMEM((1, tok), F32),
+            pltpu.VMEM((top, tok), F32),
+            pltpu.VMEM((1, dl), F32),
+            pltpu.VMEM((1, dl), F32),
+            dma((7,)),
             pltpu.VMEM((n_x, dl, 2 * cols), BF16),
             pltpu.VMEM((ff, dl), BF16),
             pltpu.VMEM((tok, dl), BF16),

time: 112 us -> 109 us (0.973); the launches traced: 110 us -> 109 us
    pallas_call x1, Pallas kernels: 109 us -> 108 us  [local(): pl.pallas_call(functools.partial(kernel, (n_z, n_x, groups, dl * n_x)), o...]
where the time goes in v3:
time: 109 us
  Pallas kernels  108 us (99%)
  local copies, waits for them, and re-layouts  1.47 us (1%)
    pallas_call x1, Pallas kernels, local(): pl.pallas_call(functools.partial(kernel, (n_z, n_x, groups, dl * n_x)), o...  108 us

profile of v3, /device:TPU:80, one launch (start us, length us, event | category | flops | bytes accessed | tf_op | source)
XLA Modules:
  0.0 109.0 jit_solution(17169934979987561472)
XLA Ops:
  0.0 107.5 %shard_map.100 = bf16[64,512]{1,0:T(8,128)(2,1)} custom-call(bf16[64,512]{1,0:T(8,128)(2,1)} %tokens_hbm.1, s32[1,64]{1,0:T(1,128)} %bitcast.10, s32[4,64]{1,0:T(4,128)} %bitcast.6, f32[1,64]{1,0:T(1,128)} %bitcast.11, f32[4,64]{1,0:T(4,128)} %bitcast.7, f32[1,512]{1,0:T(1,128)} %bitcast.8, f32[1,512]{1,0:T(1,128)} %bitcast.9, bf16[1,512,1024]{2,1,0:T(8,128)(2,1)} %wg_ref.1, ...), custom_call_target="tpu_custom_call" | custom-call | tf_op jit(solution)/shard_map/pallas_call | solution.py:533
  107.5 1.5 %copy.12 = bf16[64,512]{1,0:T(8,128)(2,1)} copy(bf16[64,512]{1,0:T(8,128)(2,1)} %shard_map.100) | data formatting | bytes 131072

commit v4 on v3

--- a/solution.py
+++ b/solution.py
@@ -13,7 +13,8 @@
 MESH = pl.DeviceIdType.MESH
 
 CHUNKS = (4, 4, 4, 4)
-START = (0, 1, 1, 1)
+ORDER = (0, 3, 1, 2)
+START = (0, 2, 2, 1)
 DIRECT = ()
 
 
@@ -471,7 +472,7 @@
 
     ends = [half + 2 if c in DIRECT else 2 * half + 1 for c in range(n_chunks)]
     total_steps = max(START[c] + ends[c] for c in range(n_chunks)) + 1
-    for c in range(n_chunks):
+    for c in ORDER:
         if START[c] == 0:
             with jax.named_scope(f"take#c={c}"):
                 take(c)
@@ -479,17 +480,18 @@
         await_bytes(wgu, w_sem.at[0])
         await_bytes(wdn, w_sem.at[1])
     for t in range(total_steps):
-        for c in range(n_chunks):
+        for c in ORDER:
             k = t - START[c]
             if 0 <= k <= ends[c]:
                 with jax.named_scope(f"stage#c={c}#k={k}"):
                     stage(c, k)
-            if k == -1:
-                with jax.named_scope(f"take#c={c}"):
-                    take(c)
         if t == 1:
             with jax.named_scope("make_meta"):
                 make_meta()
+        for c in ORDER:
+            if t == START[c] - 1:
+                with jax.named_scope(f"take#c={c}"):
+                    take(c)
     with jax.named_scope("returned"):
         gather_returned()
     with jax.named_scope("write"):

time: 109 us -> 108 us (level)
  no operation moved by 1% of the time
where the time goes in v4:
time: 108 us
  Pallas kernels  107 us (99%)
  local copies, waits for them, and re-layouts  1.47 us (1%)
    pallas_call x1, Pallas kernels, local(): pl.pallas_call(functools.partial(kernel, (n_z, n_x, groups, dl * n_x)), o...  107 us

profile of v4, /device:TPU:80, one launch (start us, length us, event | category | flops | bytes accessed | tf_op | source)
XLA Modules:
  0.0 108.0 jit_solution(14434075421850442142)
XLA Ops:
  0.0 106.6 %shard_map.100 = bf16[64,512]{1,0:T(8,128)(2,1)} custom-call(bf16[64,512]{1,0:T(8,128)(2,1)} %tokens_hbm.1, s32[1,64]{1,0:T(1,128)} %bitcast.10, s32[4,64]{1,0:T(4,128)} %bitcast.6, f32[1,64]{1,0:T(1,128)} %bitcast.11, f32[4,64]{1,0:T(4,128)} %bitcast.7, f32[1,512]{1,0:T(1,128)} %bitcast.8, f32[1,512]{1,0:T(1,128)} %bitcast.9, bf16[1,512,1024]{2,1,0:T(8,128)(2,1)} %wg_ref.1, ...), custom_call_target="tpu_custom_call" | custom-call | tf_op jit(solution)/shard_map/pallas_call | solution.py:535
  106.6 1.5 %copy.12 = bf16[64,512]{1,0:T(8,128)(2,1)} copy(bf16[64,512]{1,0:T(8,128)(2,1)} %shard_map.100) | data formatting | bytes 131072

commit v5 on v4

--- a/solution.py
+++ b/solution.py
@@ -13,7 +13,7 @@
 MESH = pl.DeviceIdType.MESH
 
 CHUNKS = (4, 4, 4, 4)
-ORDER = (0, 3, 1, 2)
+ORDER = (0, 3, 2, 1)
 START = (0, 2, 2, 1)
 DIRECT = ()
 

time: 108 us -> 108 us (level)
  no operation moved by 1% of the time
where the time goes in v5:
time: 108 us
  Pallas kernels  107 us (99%)
  local copies, waits for them, and re-layouts  1.47 us (1%)
    pallas_call x1, Pallas kernels, local(): pl.pallas_call(functools.partial(kernel, (n_z, n_x, groups, dl * n_x)), o...  107 us

profile of v5, /device:TPU:80, one launch (start us, length us, event | category | flops | bytes accessed | tf_op | source)
XLA Modules:
  0.0 108.0 jit_solution(13612541968346070595)
XLA Ops:
  0.0 106.6 %shard_map.100 = bf16[64,512]{1,0:T(8,128)(2,1)} custom-call(bf16[64,512]{1,0:T(8,128)(2,1)} %tokens_hbm.1, s32[1,64]{1,0:T(1,128)} %bitcast.10, s32[4,64]{1,0:T(4,128)} %bitcast.6, f32[1,64]{1,0:T(1,128)} %bitcast.11, f32[4,64]{1,0:T(4,128)} %bitcast.7, f32[1,512]{1,0:T(1,128)} %bitcast.8, f32[1,512]{1,0:T(1,128)} %bitcast.9, bf16[1,512,1024]{2,1,0:T(8,128)(2,1)} %wg_ref.1, ...), custom_call_target="tpu_custom_call" | custom-call | tf_op jit(solution)/shard_map/pallas_call | solution.py:535
  106.6 1.5 %copy.12 = bf16[64,512]{1,0:T(8,128)(2,1)} copy(bf16[64,512]{1,0:T(8,128)(2,1)} %shard_map.100) | data formatting | bytes 131072
